TPU v7x, 32 devices: a whole 2x2x4 slice. The times are simulated.
32 devices in a mesh: grp: 2 (over x), ep: 8 (over z, y), tp: 2 (over core).
Axes of the slice: x: 2, y: 2, z: 4, core: 2. Of those that a mesh axis runs over, the one named last changes fastest.
Arguments:
- tokens: bfloat16 [4096, 2048], P(('grp', 'ep')), parts along dimension 0, may hold values from -6 to 6
- picks: int32 [8, 512], P(None, ('grp', 'ep')), parts along dimension 1, may hold values from 0 to 2047, as said below
- route_weights: bfloat16 [8, 512], P(None, ('grp', 'ep')), parts along dimension 1, may hold values from 0.19921875 to 1
- gate_weight: bfloat16 [8, 2048, 1024], P('ep', None, 'tp'), may hold values from -0.125 to 0.125
- up_weight: bfloat16 [8, 2048, 1024], P('ep', None, 'tp'), may hold values from -0.125 to 0.125
- down_weight: bfloat16 [8, 1024, 2048], P('ep', 'tp'), may hold values from -0.1875 to 0.1875
Outputs:
- mixed: bfloat16 [4096, 2048], P(('grp', 'ep'), 'tp'), parts along dimension 0
There are 2 independent parts, one for each index of `grp`. A program takes and returns all parts, laid end to end along the dimension named above; an argument that names none is the same for every part. Nothing has to cross between parts.
Inputs may be any that keep to these rules, and one draw needn't show every extreme that they name: `picks`: slots k * 32 to (k + 1) * 32 - 1 of every expert name 32 different tokens of the block k * 256 to (k + 1) * 256 - 1.
All inputs are finite; a program needn't handle non-finite values.
Results may differ from a plain program's by a relative error of at most 0.0066.
Values may be sent and summed in bfloat16 or wider, within the bound.
A program may use at most 64 MiB of HBM per device.

v0:
```python
import jax
import jax.numpy as jnp
from jax import lax
from jax.sharding import PartitionSpec as P

TOK_DEV = 256


def per_device(tokens, picks, route_weights, gate_weight, up_weight, down_weight):
    experts, per = picks.shape
    width = tokens.shape[1]
    owners = lax.axis_size("ep")
    exp_dev = experts // owners
    local_ids = picks % TOK_DEV
    half = per // 2
    offset = lax.axis_index("tp") * half
    ids_half = lax.dynamic_slice_in_dim(local_ids, offset, half, 1)
    weights_half = lax.dynamic_slice_in_dim(route_weights, offset, half, 1)
    rows = jnp.take(tokens, ids_half, axis=0)
    got_rows, got_weights = (
        lax.all_to_all(rows, "ep", split_axis=0, concat_axis=1, tiled=True),
        lax.all_to_all(weights_half, "ep", split_axis=0, concat_axis=1, tiled=True),
    )
    got_rows = got_rows.reshape(exp_dev, owners, half, width)
    got_weights = got_weights.reshape(exp_dev, owners, half)
    got_rows, got_weights = (
        lax.all_gather(got_rows, "tp", axis=2, tiled=True),
        lax.all_gather(got_weights, "tp", axis=2, tiled=True),
    )
    got_rows = got_rows.reshape(exp_dev, owners * per, width)
    got_weights = got_weights.reshape(exp_dev, owners * per)
    gate = jnp.einsum("ecd,edf->ecf", got_rows, gate_weight, preferred_element_type=jnp.float32)
    up = jnp.einsum("ecd,edf->ecf", got_rows, up_weight, preferred_element_type=jnp.float32)
    hidden = (jax.nn.silu(gate) * up * got_weights.astype(jnp.float32)[:, :, None]).astype(
        jnp.bfloat16
    )
    partial_value = jnp.einsum(
        "ecf,efd->ecd", hidden, down_weight, preferred_element_type=jnp.float32
    ).astype(jnp.bfloat16)
    summed = lax.psum_scatter(partial_value, "tp", scatter_dimension=2, tiled=True).astype(
        jnp.float32
    )
    result = summed.astype(jnp.bfloat16)
    returned = lax.all_to_all(result, "ep", split_axis=1, concat_axis=0, tiled=True)
    flat = returned.reshape(experts * per, returned.shape[2])
    positions = lax.broadcasted_iota(jnp.int32, (TOK_DEV, experts * per), 0)
    onehot = (positions == local_ids.reshape(1, experts * per)).astype(jnp.bfloat16)
    mixed = jnp.dot(onehot, flat, preferred_element_type=jnp.float32)
    return mixed.astype(jnp.bfloat16)


def solution(mesh):
    return jax.shard_map(
        per_device,
        mesh=mesh,
        in_specs=(
            P(("grp", "ep"), None),
            P(None, ("grp", "ep")),
            P(None, ("grp", "ep")),
            P("ep", None, "tp"),
            P("ep", None, "tp"),
            P("ep", "tp", None),
        ),
        out_specs=P(("grp", "ep"), "tp"),
        check_vma=False,
    )
```

profile of v0, /device:TPU:0, one launch (start us, length us, event | category | flops | bytes accessed | tf_op | source)
XLA Modules:
  0.0 98.2 jit_solution(8991569810901540255)
XLA Ops:
  6.5 0.0 copy-start
  6.5 0.0 all-gather.4.cloned.1.call-start
  6.5 0.8 add_select_fusion
  7.4 0.1 compare_and_fusion
  7.5 0.1 reshape.84
  7.6 2.8 %gather_fusion = bf16[128,2048]{1,0:T(8,128)(2,1)S(1)} fusion(bf16[256,2048]{1,0:T(8,128)(2,1)} %param.6, s32[1024]{0:T(1024)S(1)} %pad_clamp_fusion), kind=kCustom, calls=%fused_computation | custom fusion | bytes 1049088 | tf_op jit(solution)/shard_map/jit(_take)/gather | solution.py:19
  10.4 0.0 copy-start.1
  10.4 0.1 broadcast_select_fusion
  10.5 21.7 %all_to_all.31 = bf16[8,16,2048]{2,1,0:T(8,128)(2,1)} all-to-all(bf16[8,16,2048]{2,1,0:T(8,128)(2,1)S(1)} %broadcast_select_fusion), channel_id=1, replica_groups=mesh['grp'=2,'ep'=8,'tp'=2] {'ep'}, dimensions={0} | all-to-all | bytes 1048576 | tf_op jit(solution)/shard_map/all_to_all | solution.py:21
  32.2 0.0 all-gather.4.cloned.1.call-update
  32.3 0.0 reduce-scatter.2.cloned.1.call-start
  32.3 0.0 copy-done.1
  32.3 0.1 dynamic-slice_bitcast_fusion
  32.4 9.9 %all_to_all.32 = bf16[8,1,16]{2,1,0:T(2,128)(2,1)S(1)} all-to-all(bf16[8,1,16]{2,1,0:T(2,128)(2,1)S(1)} %copy.14), channel_id=1, replica_groups=mesh['grp'=2,'ep'=8,'tp'=2] {'ep'}, dimensions={0} | all-to-all | bytes 512 | tf_op jit(solution)/shard_map/all_to_all | solution.py:22
  42.3 0.1 copy.15
  42.4 1.8 %all-gather.1 = bf16[8,1,32]{0,1,2:T(2,128)(2,1)S(1)} all-gather(bf16[8,1,16]{0,1,2:T(2,128)(2,1)S(1)} %copy.15), channel_id=3, replica_groups=mesh['grp'=2,'ep'=8,'tp'=2] {'tp'}, dimensions={2}, use_global_device_ids=true | all-gather | bytes 768 | tf_op jit(solution)/shard_map/all_gather | solution.py:28
  44.2 0.1 copy.16
  44.3 0.1 reshape.81
  44.3 3.5 %fusion.4 = f32[256,512]{1,0:T(8,128)} fusion(bf16[256,2048]{1,0:T(8,128)(2,1)} %bitcast.37, bf16[1,2048,512]{2,1,0:T(8,128)(2,1)} %param.9), kind=kOutput, calls=%fused_computation.6 | convolution fusion | flops 536870912 | bytes 3670016 | tf_op jit(solution)/shard_map/ecd,edf->ecf/dot_general | solution.py:32
  47.8 0.0 copy-done
  47.9 4.0 %fusion = bf16[1,256,2048]{2,1,0:T(8,128)(2,1)} fusion(bf16[1,512,2048]{2,1,0:T(8,128)(2,1)S(1)} %copy-done, bf16[256,2048]{1,0:T(8,128)(2,1)S(1)} %bitcast.38, bf16[1,2048,512]{2,1,0:T(8,128)(2,1)} %param.10, f32[256,512]{1,0:T(8,128)} %fusion.4, f32[256]{0:T(256)S(1)} %reshape.81), kind=kOutput, calls=%fused_computation.2 | convolution fusion | flops 1075183616 | bytes 6816768 | tf_op jit(solution)/shard_map/ecf,efd->ecd/dot_general | solution.py:37
  51.9 0.0 reduce-scatter.2.cloned.1.call-update
  51.9 5.8 %reduce-scatter.2.cloned.1.call-done = bf16[1,256,1024]{2,1,0:T(8,128)(2,1)} async-done(((bf16[1,256,2048]{2,1,0:T(8,128)(2,1)}), bf16[1,256,1024]{2,1,0:T(8,128)(2,1)}) %reduce-scatter.2.cloned.1.call-update) | async-done | bytes 524304 | tf_op jit(solution)/shard_map/reduce_scatter | solution.py:40
  57.7 1.9 %copy.24 = bf16[1,256,1024]{2,0,1:T(2,128)(2,1)S(1)} copy(bf16[1,256,1024]{2,1,0:T(8,128)(2,1)} %reduce-scatter.2.cloned.1.call-done) | data formatting | bytes 1048576 | tf_op jit(solution)/shard_map/reduce_scatter | solution.py:40
  59.6 0.6 broadcast.21
  60.2 4.8 %reduce = bf16[256,1024]{1,0:T(8,128)(2,1)} reduce(bf16[256,1,1024]{2,1,0:T(2,128)(2,1)S(1)} %bitcast.34, bf16[]{:T(256)} %broadcast.21), dimensions={1}, to_apply=%bitcast.33.reduce_sub_computation | reduce | bytes 1048578
  65.0 2.2 %reshape.97 = bf16[8,2,16384]{2,1,0:T(2,128)(2,1)} reshape(bf16[256,1024]{1,0:T(8,128)(2,1)} %reduce) | data formatting | bytes 1048576
  67.2 5.8 %all-to-all-start.2 = ((bf16[8,2,16384]{2,1,0:T(2,128)(2,1)}), bf16[8,2,16384]{2,1,0:T(2,128)(2,1)}, u32[]{:S(2)}, u32[]{:S(2)}) async-start(bf16[8,2,16384]{2,1,0:T(2,128)(2,1)} %reshape.97), calls=%async_computation.3 | async-start | bytes 1048576 | tf_op jit(solution)/shard_map/all_to_all | solution.py:44
  73.0 0.1 eq.12
  73.0 15.0 %all-to-all-done.2 = bf16[8,2,16384]{2,1,0:T(2,128)(2,1)} async-done(((bf16[8,2,16384]{2,1,0:T(2,128)(2,1)}), bf16[8,2,16384]{2,1,0:T(2,128)(2,1)}, u32[]{:S(2)}, u32[]{:S(2)}) %all-to-all-start.2) | async-done | bytes 524320 | tf_op jit(solution)/shard_map/all_to_all | solution.py:44
  88.0 2.2 %reshape.98 = bf16[256,1,1024]{2,1,0:T(2,128)(2,1)S(1)} reshape(bf16[8,2,16384]{2,1,0:T(2,128)(2,1)} %all-to-all-done.2) | data formatting | bytes 1048576
  90.3 1.2 %convolution_convert_fusion.1 = bf16[256,1024]{1,0:T(8,128)(2,1)} fusion(bf16[1,256,1024]{2,0,1:T(2,128)(2,1)S(1)} %bitcast.35, s32[256]{0:T(256)S(1)} %eq.12), kind=kOutput, calls=%fused_computation.8 | convolution fusion | flops 134545408 | bytes 1049600 | tf_op jit(solution)/shard_map/dot_general | solution.py:48
  (5 shorter events, 0.0 us)
Async XLA Ops:
  6.5 41.3 %copy-start = (bf16[1,512,2048]{2,1,0:T(8,128)(2,1)S(1)}, bf16[1,512,2048]{2,1,0:T(8,128)(2,1)}, u32[]{:S(2)}) copy-start(bf16[1,512,2048]{2,1,0:T(8,128)(2,1)} %param.11) | copy-start | bytes 6291460
  6.5 37.8 %all-gather.4.cloned.1.call-start = ((), (), s32[]{:S(2)}) async-start(), calls=%async_computation.5 | async-start | bytes 1572864 | tf_op jit(solution)/shard_map/all_gather | solution.py:27
  10.4 22.0 %copy-start.1 = (bf16[8,32]{1,0:T(8,128)(2,1)S(1)}, bf16[8,32]{1,0:T(8,128)(2,1)}, u32[]{:S(2)}) copy-start(bf16[8,32]{1,0:T(8,128)(2,1)} %param.8) | copy-start | bytes 1540
  32.3 25.5 %reduce-scatter.2.cloned.1.call-start = ((), (), s32[]{:S(2)}) async-start(), calls=%async_computation.4 | async-start | bytes 1572864 | tf_op jit(solution)/shard_map/reduce_scatter | solution.py:40
  44.3 3.5 %copy-start.2 = (bf16[8,32,2048]{2,1,0:T(8,128)(2,1)S(1)}, bf16[8,32,2048]{2,1,0:T(8,128)(2,1)}, u32[]{:S(2)}) copy-start(bf16[8,32,2048]{2,1,0:T(8,128)(2,1)} %all-gather.4.cloned.1.call-done) | copy-start | bytes 3145732
  67.2 20.8 %all-to-all-start.2 = ((bf16[8,2,16384]{2,1,0:T(2,128)(2,1)}), bf16[8,2,16384]{2,1,0:T(2,128)(2,1)}, u32[]{:S(2)}, u32[]{:S(2)}) async-start(bf16[8,2,16384]{2,1,0:T(2,128)(2,1)} %reshape.97), calls=%async_computation.3 | async-start | bytes 1048576 | tf_op jit(solution)/shard_map/all_to_all | solution.py:44
Sparse Core Ops, SparseCore 0:
  32.4 8.0 all-gather.3
  52.0 5.6 reduce-scatter.1
where the time goes:
time: 98.7 us; the launch traced here: 98.2 us
  blocking collectives  33.4 us (34%)
  waiting for transfers between devices  20.9 us (21%)
  between operations  13.5 us (14%)
  local copies, waits for them, and re-layouts  10.2 us (10%)
  matrix products  8.68 us (9%)
  other arithmetic  5.83 us (6%)
  starting transfers between devices  5.8 us (6%)
    all_to_all x1, blocking collectives, per_device(): lax.all_to_all(rows, 'ep', split_axis=0, concat_axis=1, tiled=True)  21.7 us
    all_to_all x1, waiting for transfers between devices, per_device(): lax.all_to_all(result, 'ep', split_axis=1, concat_axis=0, tiled=True)  15 us
    all_to_all x1, blocking collectives, per_device(): lax.all_to_all(weights_half, 'ep', split_axis=0, concat_axis=1, tiled=True)  9.87 us
    reduce_scatter x1, waiting for transfers between devices, per_device(): lax.psum_scatter(partial_value, 'tp', scatter_dimension=2, tiled=True)  5.84 us
    all_to_all x1, starting transfers between devices, per_device(): lax.all_to_all(result, 'ep', split_axis=1, concat_axis=0, tiled=True)  5.76 us
    unnamed x9, local copies, waits for them, and re-layouts  5.05 us
    unnamed x1, other arithmetic  4.78 us
    dot_general x1, matrix products, per_device(): jnp.einsum('ecf,efd->ecd', hidden, down_weight, preferred_element_type=jn...  4.03 us
  transfers between devices with their start and end apart: 3, of which 2 were waited for; matrix products, arithmetic and copies ran while one was open for 0% of the time, Pallas kernels for 0%

commit v1 on v0

v1 whole, which is shorter than its diff:
```python
import functools

import jax
import jax.numpy as jnp
from jax import lax
from jax.experimental import pallas as pl
from jax.experimental.pallas import tpu as pltpu
from jax.sharding import PartitionSpec as P

MESH = pl.DeviceIdType.MESH
F32 = jnp.float32
BF16 = jnp.bfloat16


def flip(me, k):
    bit, out = 1, me
    while bit <= k:
        if k & bit:
            out = out + bit * (1 - 2 * ((me // bit) % 2))
        bit *= 2
    return out


def groups_of(n):
    if n < 4:
        return [list(range(n))]
    half, quarter = n // 2, n // 4
    return [
        list(range(half, half + quarter)),
        list(range(half)),
        list(range(half + quarter, n)),
    ]


def kernel(
    n, per, groups,
    tokens_hbm, ids_ref, half_ids_ref, route_ref, gate_hbm, up_hbm, down_hbm, out_ref,
    tokens, gate_w, up_w, down_w, outgoing, rows, mine, part_out, part_in, result, returned,
    load_sem, disp_send, disp_recv, fwd_send, fwd_recv, part_send, part_recv, ret_send, ret_recv,
):
    me, core = lax.axis_index("ep"), lax.axis_index("tp")
    other = 1 - core
    half = per // 2
    tok, width = tokens.shape
    cols = width // 2
    order = [k for g in groups for k in g]
    place = {k: i for i, k in enumerate(order)}

    loads = [
        pltpu.make_async_copy(src, dst, load_sem.at[i])
        for i, (src, dst) in enumerate(
            ((tokens_hbm, tokens), (gate_hbm.at[0], gate_w), (up_hbm.at[0], up_w), (down_hbm.at[0], down_w))
        )
    ]
    for load in loads:
        load.start()

    barrier = pltpu.get_barrier_semaphore()
    for k in order:
        if k:
            pl.semaphore_signal(barrier, inc=1, device_id={"ep": flip(me, k)}, device_id_type=MESH)
    pl.semaphore_signal(barrier, inc=1, device_id={"tp": other}, device_id_type=MESH)

    ids = jnp.where(core == 0, half_ids_ref[0:1, :], half_ids_ref[1:2, :])
    spots = lax.broadcasted_iota(jnp.int32, (tok, n * half), 0)
    pick = jnp.where(spots == ids, 1.0, 0.0).astype(BF16)
    loads[0].wait()
    outgoing[...] = lax.dot_general(
        pick, tokens[...], (((0,), (0,)), ((), ())), preferred_element_type=F32
    ).astype(BF16)

    def spot(k):
        return pl.ds(place[k] * per + pl.multiple_of(core * half, half), half)

    def dispatch(k):
        peer = flip(me, k)
        return pltpu.make_async_remote_copy(
            outgoing.at[pl.ds(pl.multiple_of(peer * half, half), half)], rows.at[spot(k)],
            disp_send.at[k], disp_recv.at[k], device_id={"ep": peer}, device_id_type=MESH,
        )

    def forward(k):
        src = rows.at[spot(k)] if k else outgoing.at[pl.ds(pl.multiple_of(me * half, half), half)]
        return pltpu.make_async_remote_copy(
            src, rows.at[spot(k)], fwd_send.at[k], fwd_recv.at[k], device_id={"tp": other}, device_id_type=MESH,
        )

    def swap(g):
        at = pl.ds(place[groups[g][0]] * per, len(groups[g]) * per)
        return pltpu.make_async_remote_copy(
            part_out.at[at], part_in.at[at], part_send.at[g], part_recv.at[g],
            device_id={"tp": other}, device_id_type=MESH,
        )

    def giveback(k):
        return pltpu.make_async_remote_copy(
            result.at[pl.ds(place[k] * per, per)], returned.at[pl.ds(pl.multiple_of(me * per, per), per)],
            ret_send.at[k], ret_recv.at[k], device_id={"ep": flip(me, k)}, device_id_type=MESH,
        )

    pl.semaphore_wait(barrier, n)
    for k in order:
        if k:
            dispatch(k).start()
    forward(0).start()
    rows[spot(0), :] = outgoing[pl.ds(pl.multiple_of(me * half, half), half), :]

    def relay(g):
        for k in groups[g]:
            if k:
                dispatch(k).wait_recv()
                forward(k).start()

    def compute(g):
        for k in groups[g]:
            forward(k).wait_recv()
        if g == 0:
            for load in loads[1:]:
                load.wait()
        count = len(groups[g]) * per
        at = pl.ds(place[groups[g][0]] * per, count)
        x = rows[at, :]
        gate = jnp.dot(x, gate_w[...], preferred_element_type=F32)
        up = jnp.dot(x, up_w[...], preferred_element_type=F32)
        hidden = (gate / (1.0 + jnp.exp(-gate)) * up).astype(BF16)
        theirs = down_w[:, pl.ds(pl.multiple_of(other * cols, cols), cols)]
        part_out[at, :] = jnp.dot(hidden, theirs, preferred_element_type=F32).astype(BF16)
        swap(g).start()
        ours = down_w[:, pl.ds(pl.multiple_of(core * cols, cols), cols)]
        mine[at, :] = jnp.dot(hidden, ours, preferred_element_type=F32)

    def finish(g):
        swap(g).wait_recv()
        at = pl.ds(place[groups[g][0]] * per, len(groups[g]) * per)
        result[at, :] = (mine[at, :] + part_in[at, :].astype(F32)).astype(BF16)
        for k in groups[g]:
            if k:
                giveback(k).start()
            else:
                returned[pl.ds(pl.multiple_of(me * per, per), per), :] = result[pl.ds(place[k] * per, per), :]

    for g in range(len(groups)):
        relay(g)
        if g:
            finish(g - 1)
        compute(g)
    finish(len(groups) - 1)

    ids_all = ids_ref[...]
    spots_all = lax.broadcasted_iota(jnp.int32, (tok, n * per), 0)
    combine = jnp.where(spots_all == ids_all, route_ref[...].astype(F32), 0.0).astype(BF16)
    for k in order:
        if k:
            giveback(k).wait_recv()
    out_ref[...] = jnp.dot(combine, returned[...], preferred_element_type=F32).astype(BF16)
    for k in order:
        if k:
            dispatch(k).wait_send()
            giveback(k).wait_send()
        forward(k).wait_send()
    for g in range(len(groups)):
        swap(g).wait_send()


def per_device(tokens, picks, route_weights, gate_weight, up_weight, down_weight):
    n = lax.axis_size("ep")
    experts, per = picks.shape
    tok, width = tokens.shape
    hidden = gate_weight.shape[2]
    slots, cols = n * per, width // 2
    groups = groups_of(n)
    local = picks - lax.axis_index("ep") * tok
    half_ids = local.reshape(n, 2, per // 2).transpose(1, 0, 2).reshape(2, slots // 2)
    any_spec, vmem_spec = pl.BlockSpec(memory_space=pl.ANY), pl.BlockSpec(memory_space=pltpu.VMEM)
    dma = pltpu.SemaphoreType.DMA
    return pl.pallas_call(
        functools.partial(kernel, n, per, groups),
        out_shape=jax.ShapeDtypeStruct((tok, cols), BF16),
        in_specs=[any_spec, vmem_spec, vmem_spec, vmem_spec, any_spec, any_spec, any_spec],
        out_specs=vmem_spec,
        scratch_shapes=[
            pltpu.VMEM((tok, width), BF16),
            pltpu.VMEM((width, hidden), BF16),
            pltpu.VMEM((width, hidden), BF16),
            pltpu.VMEM((hidden, width), BF16),
            pltpu.VMEM((slots // 2, width), BF16),
            pltpu.VMEM((slots, width), BF16),
            pltpu.VMEM((slots, cols), F32),
            pltpu.VMEM((slots, cols), BF16),
            pltpu.VMEM((slots, cols), BF16),
            pltpu.VMEM((slots, cols), BF16),
            pltpu.VMEM((slots, cols), BF16),
            dma((4,)),
            dma((n,)), dma((n,)), dma((n,)), dma((n,)),
            dma((len(groups),)), dma((len(groups),)),
            dma((n,)), dma((n,)),
        ],
        compiler_params=pltpu.CompilerParams(
            collective_id=0, has_side_effects=True, vmem_limit_bytes=60 * 1024 * 1024
        ),
    )(
        tokens, local.reshape(1, slots), half_ids, route_weights.reshape(1, slots),
        gate_weight, up_weight, down_weight,
    )


def solution(mesh):
    return jax.shard_map(
        per_device,
        mesh=mesh,
        in_specs=(
            P(("grp", "ep"), None),
            P(None, ("grp", "ep")),
            P(None, ("grp", "ep")),
            P("ep", None, "tp"),
            P("ep", None, "tp"),
            P("ep", "tp", None),
        ),
        out_specs=P(("grp", "ep"), "tp"),
        check_vma=False,
    )
```

time: 98.7 us -> 38.1 us (0.39)
  blocking collectives: 33.4 us -> 0 us
  Pallas kernels: 0 us -> 32.5 us
  waiting for transfers between devices: 20.9 us -> 0 us
  between operations: 13.5 us -> 0.01 us
  matrix products: 8.68 us -> 0 us
  starting transfers between devices: 5.8 us -> 0 us
  local copies, waits for them, and re-layouts: 10.2 us -> 4.58 us
  other arithmetic: 5.83 us -> 0.69 us
    pallas_call x0 -> x1, Pallas kernels: none -> 32.5 us  [per_device(): pl.pallas_call(functools.partial(kernel, n, per, groups), out_shape=jax.S...]
    all_to_all x2 -> x0, blocking collectives: 31.6 us -> none  [the longest x1 21.7 us: per_device(): lax.all_to_all(rows, 'ep', split_axis=0, concat_axis=1, tiled=True)]
    all_to_all x1 -> x0, waiting for transfers between devices: 15 us -> none  [per_device(): lax.all_to_all(result, 'ep', split_axis=1, concat_axis=0, tiled=True)]
    dot_general x3 -> x0, matrix products: 8.68 us -> none  [the longest x1 4.03 us: per_device(): jnp.einsum('ecf,efd->ecd', hidden, down_weight, preferred_element_type=jn...]
    reduce_scatter x1 -> x0, waiting for transfers between devices: 5.84 us -> none  [per_device(): lax.psum_scatter(partial_value, 'tp', scatter_dimension=2, tiled=True)]
    all_to_all x1 -> x0, starting transfers between devices: 5.76 us -> none  [per_device(): lax.all_to_all(result, 'ep', split_axis=1, concat_axis=0, tiled=True)]
    unnamed x1 -> x0, other arithmetic: 4.78 us -> none
    unnamed x9 -> x1, local copies, waits for them, and re-layouts: 5.05 us -> 1.87 us
  transfers between devices with their start and end apart: 3 -> 0, of which waited for: 2 -> 0; matrix products, arithmetic and copies ran while one was open for 0% -> 0% of each run, Pallas kernels for 0% -> 0%
where the time goes in v1:
time: 38.1 us; the launch traced here: 37.8 us
  Pallas kernels  32.5 us (85%)
  local copies, waits for them, and re-layouts  4.58 us (12%)
  other arithmetic  0.69 us (2%)
    pallas_call x1, Pallas kernels, per_device(): pl.pallas_call(functools.partial(kernel, n, per, groups), out_shape=jax.S...  32.5 us
    unnamed x1, local copies, waits for them, and re-layouts  1.87 us
    reshape x1, local copies, waits for them, and re-layouts, per_device(): route_weights.reshape(1, slots)  1.31 us

profile of v1, /device:TPU:0, one launch (start us, length us, event | category | flops | bytes accessed | tf_op | source)
XLA Modules:
  0.0 37.8 jit_solution(16406597746519441463)
XLA Ops:
  0.0 1.3 %reshape.15.route_ref = bf16[1,256]{1,0:T(2,128)(2,1)} reshape(bf16[8,32]{1,0:T(8,128)(2,1)} %param.8) | data formatting | bytes 1024 | tf_op jit(solution)/shard_map/reshape | solution.py:202
  1.3 0.7 %broadcast_subtract_fusion = s32[8,32]{1,0:T(8,128)S(1)} fusion(s32[8,32]{1,0:T(8,128)} %param.7, s32[]{:T(128)S(6)} %mul.3), kind=kLoop, calls=%fused_computation.1 | loop fusion | flops 256 | bytes 2052 | tf_op jit(solution)/shard_map/sub | solution.py:172
  2.0 0.6 %reshape.12.ids_ref = s32[1,256]{1,0:T(1,128)} reshape(s32[8,32]{1,0:T(8,128)S(1)} %broadcast_subtract_fusion) | data formatting | bytes 2048 | tf_op jit(solution)/shard_map/reshape | solution.py:202
  2.6 0.1 reshape.13
  2.7 0.7 %reshape.14.half_ids_ref = s32[2,128]{1,0:T(2,128)} reshape(s32[2,8,16]{2,1,0:T(8,128)S(1)} %bitcast.3) | data formatting | bytes 2048 | tf_op jit(solution)/shard_map/reshape | solution.py:173
  3.4 32.5 %shard_map.64 = bf16[256,1024]{1,0:T(8,128)(2,1)} custom-call(bf16[256,2048]{1,0:T(8,128)(2,1)} %tokens_hbm.1, s32[1,256]{1,0:T(1,128)} %reshape.12.ids_ref, s32[2,128]{1,0:T(2,128)} %reshape.14.half_ids_ref, bf16[1,256]{1,0:T(2,128)(2,1)} %reshape.15.route_ref, bf16[1,2048,512]{2,1,0:T(8,128)(2,1)} %gate_hbm.1, bf16[1,2048,512]{2,1,0:T(8,128)(2,1)} %up_hbm.1, ...), custom_call_target="tpu_custom_call" | custom-call | tf_op jit(solution)/shard_map/pallas_call | solution.py:176
  35.9 1.9 %copy.11 = bf16[256,1024]{1,0:T(8,128)(2,1)} copy(bf16[256,1024]{1,0:T(8,128)(2,1)} %shard_map.64) | data formatting | bytes 1048576
  (1 shorter events, 0.0 us)

commit v2 on v1

--- a/solution.py
+++ b/solution.py
@@ -34,8 +34,8 @@
 
 def kernel(
     n, per, groups,
-    tokens_hbm, ids_ref, half_ids_ref, route_ref, gate_hbm, up_hbm, down_hbm, out_ref,
-    tokens, gate_w, up_w, down_w, outgoing, rows, mine, part_out, part_in, result, returned,
+    tokens_hbm, picks_hbm, route_hbm, gate_hbm, up_hbm, down_hbm, returned, combine,
+    tokens, picks, route, gate_w, up_w, down_w, outgoing, rows, mine, part_out, part_in, result,
     load_sem, disp_send, disp_recv, fwd_send, fwd_recv, part_send, part_recv, ret_send, ret_recv,
 ):
     me, core = lax.axis_index("ep"), lax.axis_index("tp")
@@ -49,7 +49,10 @@
     loads = [
         pltpu.make_async_copy(src, dst, load_sem.at[i])
         for i, (src, dst) in enumerate(
-            ((tokens_hbm, tokens), (gate_hbm.at[0], gate_w), (up_hbm.at[0], up_w), (down_hbm.at[0], down_w))
+            (
+                (picks_hbm, picks), (tokens_hbm, tokens), (route_hbm, route),
+                (gate_hbm.at[0], gate_w), (up_hbm.at[0], up_w), (down_hbm.at[0], down_w),
+            )
         )
     ]
     for load in loads:
@@ -61,10 +64,13 @@
             pl.semaphore_signal(barrier, inc=1, device_id={"ep": flip(me, k)}, device_id_type=MESH)
     pl.semaphore_signal(barrier, inc=1, device_id={"tp": other}, device_id_type=MESH)
 
-    ids = jnp.where(core == 0, half_ids_ref[0:1, :], half_ids_ref[1:2, :])
+    loads[0].wait()
+    local = picks[...] - me * tok
+    kept = jnp.where(core == 0, local[:, :half], local[:, half:])
+    ids = jnp.concatenate([kept[e:e + 1, :] for e in range(n)], axis=1)
     spots = lax.broadcasted_iota(jnp.int32, (tok, n * half), 0)
     pick = jnp.where(spots == ids, 1.0, 0.0).astype(BF16)
-    loads[0].wait()
+    loads[1].wait()
     outgoing[...] = lax.dot_general(
         pick, tokens[...], (((0,), (0,)), ((), ())), preferred_element_type=F32
     ).astype(BF16)
@@ -103,6 +109,12 @@
         if k:
             dispatch(k).start()
     forward(0).start()
+    loads[2].wait()
+    ids_all = jnp.concatenate([local[e:e + 1, :] for e in range(n)], axis=1)
+    weight = route[...].astype(F32)
+    weight_all = jnp.concatenate([weight[e:e + 1, :] for e in range(n)], axis=1)
+    spots_all = lax.broadcasted_iota(jnp.int32, (tok, n * per), 0)
+    combine[...] = jnp.where(spots_all == ids_all, weight_all, 0.0).astype(BF16)
     rows[spot(0), :] = outgoing[pl.ds(pl.multiple_of(me * half, half), half), :]
 
     def relay(g):
@@ -115,7 +127,7 @@
         for k in groups[g]:
             forward(k).wait_recv()
         if g == 0:
-            for load in loads[1:]:
+            for load in loads[3:]:
                 load.wait()
         count = len(groups[g]) * per
         at = pl.ds(place[groups[g][0]] * per, count)
@@ -146,13 +158,9 @@
         compute(g)
     finish(len(groups) - 1)
 
-    ids_all = ids_ref[...]
-    spots_all = lax.broadcasted_iota(jnp.int32, (tok, n * per), 0)
-    combine = jnp.where(spots_all == ids_all, route_ref[...].astype(F32), 0.0).astype(BF16)
     for k in order:
         if k:
             giveback(k).wait_recv()
-    out_ref[...] = jnp.dot(combine, returned[...], preferred_element_type=F32).astype(BF16)
     for k in order:
         if k:
             dispatch(k).wait_send()
@@ -169,17 +177,19 @@
     hidden = gate_weight.shape[2]
     slots, cols = n * per, width // 2
     groups = groups_of(n)
-    local = picks - lax.axis_index("ep") * tok
-    half_ids = local.reshape(n, 2, per // 2).transpose(1, 0, 2).reshape(2, slots // 2)
     any_spec, vmem_spec = pl.BlockSpec(memory_space=pl.ANY), pl.BlockSpec(memory_space=pltpu.VMEM)
     dma = pltpu.SemaphoreType.DMA
-    return pl.pallas_call(
+    returned, combine = pl.pallas_call(
         functools.partial(kernel, n, per, groups),
-        out_shape=jax.ShapeDtypeStruct((tok, cols), BF16),
-        in_specs=[any_spec, vmem_spec, vmem_spec, vmem_spec, any_spec, any_spec, any_spec],
-        out_specs=vmem_spec,
+        out_shape=(
+            jax.ShapeDtypeStruct((slots, cols), BF16), jax.ShapeDtypeStruct((tok, slots), BF16),
+        ),
+        in_specs=[any_spec] * 6,
+        out_specs=(vmem_spec, vmem_spec),
         scratch_shapes=[
             pltpu.VMEM((tok, width), BF16),
+            pltpu.VMEM((n, per), jnp.int32),
+            pltpu.VMEM((n, per), BF16),
             pltpu.VMEM((width, hidden), BF16),
             pltpu.VMEM((width, hidden), BF16),
             pltpu.VMEM((hidden, width), BF16),
@@ -189,8 +199,7 @@
             pltpu.VMEM((slots, cols), BF16),
             pltpu.VMEM((slots, cols), BF16),
             pltpu.VMEM((slots, cols), BF16),
-            pltpu.VMEM((slots, cols), BF16),
-            dma((4,)),
+            dma((6,)),
             dma((n,)), dma((n,)), dma((n,)), dma((n,)),
             dma((len(groups),)), dma((len(groups),)),
             dma((n,)), dma((n,)),
@@ -198,10 +207,8 @@
         compiler_params=pltpu.CompilerParams(
             collective_id=0, has_side_effects=True, vmem_limit_bytes=60 * 1024 * 1024
         ),
-    )(
-        tokens, local.reshape(1, slots), half_ids, route_weights.reshape(1, slots),
-        gate_weight, up_weight, down_weight,
-    )
+    )(tokens, picks, route_weights, gate_weight, up_weight, down_weight)
+    return jnp.dot(combine, returned, preferred_element_type=F32).astype(BF16)
 
 
 def solution(mesh):

time: 38.1 us -> 34.1 us (0.90)
  local copies, waits for them, and re-layouts: 4.58 us -> 0 us
  matrix products: 0 us -> 2.22 us
  Pallas kernels: 32.5 us -> 31.7 us
  other arithmetic: 0.69 us -> 0 us
    reshape x5 -> x0, local copies, waits for them, and re-layouts: 2.71 us -> none  [the longest x1 1.31 us: per_device(): route_weights.reshape(1, slots)]
    dot_general x0 -> x1, matrix products: none -> 2.22 us  [per_device(): return jnp.dot(combine, returned, preferred_element_type=F32).astype(BF16)]
    unnamed x1 -> x0, local copies, waits for them, and re-layouts: 1.87 us -> none
    pallas_call x1, Pallas kernels: 32.5 us -> 31.7 us  [per_device(): pl.pallas_call(functools.partial(kernel, n, per, groups), out_shape=(jax....]
    sub x1 -> x0, other arithmetic: 0.69 us -> none  [per_device(): local = picks - lax.axis_index('ep') * tok]
where the time goes in v2:
time: 34.1 us; the launch traced here: 33.9 us
  Pallas kernels  31.7 us (93%)
  matrix products  2.22 us (7%)
    pallas_call x1, Pallas kernels, per_device(): pl.pallas_call(functools.partial(kernel, n, per, groups), out_shape=(jax....  31.7 us
    dot_general x1, matrix products, per_device(): return jnp.dot(combine, returned, preferred_element_type=F32).astype(BF16)  2.22 us

profile of v2, /device:TPU:0, one launch (start us, length us, event | category | flops | bytes accessed | tf_op | source)
XLA Modules:
  0.0 33.9 jit_solution(4092233475261937420)
XLA Ops:
  0.0 31.7 %shard_map.64 = (bf16[256,1024]{1,0:T(8,128)(2,1)}, bf16[256,256]{1,0:T(8,128)(2,1)}) custom-call(bf16[256,2048]{1,0:T(8,128)(2,1)} %tokens_hbm.1, s32[8,32]{1,0:T(8,128)} %picks_hbm.1, bf16[8,32]{1,0:T(8,128)(2,1)} %route_hbm.1, bf16[1,2048,512]{2,1,0:T(8,128)(2,1)} %gate_hbm.1, bf16[1,2048,512]{2,1,0:T(8,128)(2,1)} %up_hbm.1, bf16[1,512,2048]{2,1,0:T(8,128)(2,1)} %down_hbm.1), custom_call_target="tpu_custom_call" | custom-call | tf_op jit(solution)/shard_map/pallas_call | solution.py:182
  31.7 2.2 %convolution_convert_fusion = bf16[256,1024]{1,0:T(8,128)(2,1)} fusion(bf16[256,256]{1,0:T(8,128)(2,1)} %get-tuple-element.7, bf16[256,1024]{1,0:T(8,128)(2,1)} %get-tuple-element.8), kind=kOutput, calls=%fused_computation | convolution fusion | flops 134479872 | bytes 1179648 | tf_op jit(solution)/shard_map/dot_general | solution.py:211

commit v3 on v2

--- a/solution.py
+++ b/solution.py
@@ -22,14 +22,11 @@
 
 
 def groups_of(n):
-    if n < 4:
+    if n < 8:
         return [list(range(n))]
-    half, quarter = n // 2, n // 4
-    return [
-        list(range(half, half + quarter)),
-        list(range(half)),
-        list(range(half + quarter, n)),
-    ]
+    half, eighth = n // 2, n // 8
+    far = [list(range(at, at + eighth)) for at in range(half, n, eighth)]
+    return far[:2] + [list(range(half))] + far[2:]
 
 
 def kernel(
@@ -65,15 +62,25 @@
     pl.semaphore_signal(barrier, inc=1, device_id={"tp": other}, device_id_type=MESH)
 
     loads[0].wait()
-    local = picks[...] - me * tok
-    kept = jnp.where(core == 0, local[:, :half], local[:, half:])
-    ids = jnp.concatenate([kept[e:e + 1, :] for e in range(n)], axis=1)
     spots = lax.broadcasted_iota(jnp.int32, (tok, n * half), 0)
-    pick = jnp.where(spots == ids, 1.0, 0.0).astype(BF16)
+    first = len(groups[0] + groups[1]) if len(groups) > 1 else n
+
+    def gather(ks):
+        kept = []
+        for k in ks:
+            row = picks[pl.ds(flip(me, k), 1), :] - me * tok
+            kept.append(jnp.where(core == 0, row[:, :half], row[:, half:]))
+        ids = jnp.concatenate(kept, axis=1)
+        pick = jnp.where(spots[:, :len(ks) * half] == ids, 1.0, 0.0).astype(BF16)
+        outgoing[pl.ds(place[ks[0]] * half, len(ks) * half), :] = lax.dot_general(
+            pick, tokens[...], (((0,), (0,)), ((), ())), preferred_element_type=F32
+        ).astype(BF16)
+
     loads[1].wait()
-    outgoing[...] = lax.dot_general(
-        pick, tokens[...], (((0,), (0,)), ((), ())), preferred_element_type=F32
-    ).astype(BF16)
+    gather(order[:first])
+
+    def sent(k):
+        return pl.ds(place[k] * half, half)
 
     def spot(k):
         return pl.ds(place[k] * per + pl.multiple_of(core * half, half), half)
@@ -81,12 +88,12 @@
     def dispatch(k):
         peer = flip(me, k)
         return pltpu.make_async_remote_copy(
-            outgoing.at[pl.ds(pl.multiple_of(peer * half, half), half)], rows.at[spot(k)],
+            outgoing.at[sent(k)], rows.at[spot(k)],
             disp_send.at[k], disp_recv.at[k], device_id={"ep": peer}, device_id_type=MESH,
         )
 
     def forward(k):
-        src = rows.at[spot(k)] if k else outgoing.at[pl.ds(pl.multiple_of(me * half, half), half)]
+        src = rows.at[spot(k)] if k else outgoing.at[sent(0)]
         return pltpu.make_async_remote_copy(
             src, rows.at[spot(k)], fwd_send.at[k], fwd_recv.at[k], device_id={"tp": other}, device_id_type=MESH,
         )
@@ -105,17 +112,23 @@
         )
 
     pl.semaphore_wait(barrier, n)
-    for k in order:
+    for k in order[:first]:
         if k:
             dispatch(k).start()
+    if first < n:
+        gather(order[first:])
+        for k in order[first:]:
+            if k:
+                dispatch(k).start()
     forward(0).start()
     loads[2].wait()
+    local = picks[...] - me * tok
     ids_all = jnp.concatenate([local[e:e + 1, :] for e in range(n)], axis=1)
     weight = route[...].astype(F32)
     weight_all = jnp.concatenate([weight[e:e + 1, :] for e in range(n)], axis=1)
     spots_all = lax.broadcasted_iota(jnp.int32, (tok, n * per), 0)
     combine[...] = jnp.where(spots_all == ids_all, weight_all, 0.0).astype(BF16)
-    rows[spot(0), :] = outgoing[pl.ds(pl.multiple_of(me * half, half), half), :]
+    rows[spot(0), :] = outgoing[sent(0), :]
 
     def relay(g):
         for k in groups[g]:
@@ -182,7 +195,7 @@
     returned, combine = pl.pallas_call(
         functools.partial(kernel, n, per, groups),
         out_shape=(
-            jax.ShapeDtypeStruct((slots, cols), BF16), jax.ShapeDtypeStruct((tok, slots), BF16),
+            pltpu.VMEM((slots, cols), BF16), pltpu.VMEM((tok, slots), BF16),
         ),
         in_specs=[any_spec] * 6,
         out_specs=(vmem_spec, vmem_spec),

time: 34.1 us -> 32.2 us (0.944)
  matrix products: 2.22 us -> 1.1 us
  Pallas kernels: 31.7 us -> 30.9 us
    dot_general x1, matrix products: 2.22 us -> 1.1 us  [per_device(): return jnp.dot(combine, returned, preferred_element_type=F32).astype(BF16)]
    pallas_call x1, Pallas kernels: 31.7 us -> 30.9 us  [per_device(): pl.pallas_call(functools.partial(kernel, n, per, groups), out_shape=(pltp...]
where the time goes in v3:
time: 32.2 us; the launch traced here: 32 us
  Pallas kernels  30.9 us (96%)
  matrix products  1.1 us (3%)
    pallas_call x1, Pallas kernels, per_device(): pl.pallas_call(functools.partial(kernel, n, per, groups), out_shape=(pltp...  30.9 us
    dot_general x1, matrix products, per_device(): return jnp.dot(combine, returned, preferred_element_type=F32).astype(BF16)  1.1 us

profile of v3, /device:TPU:0, one launch (start us, length us, event | category | flops | bytes accessed | tf_op | source)
XLA Modules:
  0.0 32.0 jit_solution(4520641490392379261)
XLA Ops:
  0.0 30.9 %shard_map.64 = (bf16[256,1024]{1,0:T(8,128)(2,1)S(1)}, bf16[256,256]{1,0:T(8,128)(2,1)S(1)}) custom-call(bf16[256,2048]{1,0:T(8,128)(2,1)} %tokens_hbm.1, s32[8,32]{1,0:T(8,128)} %picks_hbm.1, bf16[8,32]{1,0:T(8,128)(2,1)} %route_hbm.1, bf16[1,2048,512]{2,1,0:T(8,128)(2,1)} %gate_hbm.1, bf16[1,2048,512]{2,1,0:T(8,128)(2,1)} %up_hbm.1, ...), custom_call_target="tpu_custom_call" | custom-call | tf_op jit(solution)/shard_map/pallas_call | solution.py:195
  30.9 1.1 %convolution_convert_fusion = bf16[256,1024]{1,0:T(8,128)(2,1)} fusion(bf16[256,256]{1,0:T(8,128)(2,1)S(1)} %get-tuple-element.7, bf16[256,1024]{1,0:T(8,128)(2,1)S(1)} %get-tuple-element.8), kind=kOutput, calls=%fused_computation | convolution fusion | flops 134479872 | bytes 1179648 | tf_op jit(solution)/shard_map/dot_general | solution.py:224

commit v4 on v3

--- a/solution.py
+++ b/solution.py
@@ -23,14 +23,17 @@
 
 def groups_of(n):
     if n < 8:
-        return [list(range(n))]
-    half, eighth = n // 2, n // 8
+        return [list(range(n))], [[]], list(range(n))
+    half, quarter, eighth = n // 2, n // 4, n // 8
     far = [list(range(at, at + eighth)) for at in range(half, n, eighth)]
-    return far[:2] + [list(range(half))] + far[2:]
+    far = far[2:] + far[:2]
+    nearest, near = list(range(quarter)), list(range(quarter, half))
+    groups = [nearest, far[0], far[1], near, far[2], far[3]]
+    return groups, [[1], [2], [3], [4, 5], [], []], far[0] + far[1] + nearest + near + far[2] + far[3]
 
 
 def kernel(
-    n, per, groups,
+    n, per, groups, ahead, sending,
     tokens_hbm, picks_hbm, route_hbm, gate_hbm, up_hbm, down_hbm, returned, combine,
     tokens, picks, route, gate_w, up_w, down_w, outgoing, rows, mine, part_out, part_in, result,
     load_sem, disp_send, disp_recv, fwd_send, fwd_recv, part_send, part_recv, ret_send, ret_recv,
@@ -63,7 +66,7 @@
 
     loads[0].wait()
     spots = lax.broadcasted_iota(jnp.int32, (tok, n * half), 0)
-    first = len(groups[0] + groups[1]) if len(groups) > 1 else n
+    first = len(groups[0] + groups[1] + groups[2]) if len(groups) > 1 else n
 
     def gather(ks):
         kept = []
@@ -112,14 +115,13 @@
         )
 
     pl.semaphore_wait(barrier, n)
-    for k in order[:first]:
+    for k in sending[:first]:
         if k:
             dispatch(k).start()
     if first < n:
         gather(order[first:])
-        for k in order[first:]:
-            if k:
-                dispatch(k).start()
+        for k in sending[first:]:
+            dispatch(k).start()
     forward(0).start()
     loads[2].wait()
     local = picks[...] - me * tok
@@ -136,23 +138,29 @@
                 dispatch(k).wait_recv()
                 forward(k).start()
 
-    def compute(g):
+    def region(g):
+        return pl.ds(place[groups[g][0]] * per, len(groups[g]) * per)
+
+    def enter(g):
         for k in groups[g]:
             forward(k).wait_recv()
+        x = rows[region(g), :]
         if g == 0:
-            for load in loads[3:]:
-                load.wait()
-        count = len(groups[g]) * per
-        at = pl.ds(place[groups[g][0]] * per, count)
-        x = rows[at, :]
+            loads[3].wait()
         gate = jnp.dot(x, gate_w[...], preferred_element_type=F32)
+        if g == 0:
+            loads[4].wait()
         up = jnp.dot(x, up_w[...], preferred_element_type=F32)
-        hidden = (gate / (1.0 + jnp.exp(-gate)) * up).astype(BF16)
+        return (gate / (1.0 + jnp.exp(-gate)) * up).astype(BF16)
+
+    def leave(g, hidden):
+        if g == 0:
+            loads[5].wait()
         theirs = down_w[:, pl.ds(pl.multiple_of(other * cols, cols), cols)]
-        part_out[at, :] = jnp.dot(hidden, theirs, preferred_element_type=F32).astype(BF16)
+        part_out[region(g), :] = jnp.dot(hidden, theirs, preferred_element_type=F32).astype(BF16)
         swap(g).start()
         ours = down_w[:, pl.ds(pl.multiple_of(core * cols, cols), cols)]
-        mine[at, :] = jnp.dot(hidden, ours, preferred_element_type=F32)
+        mine[region(g), :] = jnp.dot(hidden, ours, preferred_element_type=F32)
 
     def finish(g):
         swap(g).wait_recv()
@@ -164,11 +172,14 @@
             else:
                 returned[pl.ds(pl.multiple_of(me * per, per), per), :] = result[pl.ds(place[k] * per, per), :]
 
+    relay(0)
     for g in range(len(groups)):
-        relay(g)
+        hidden = enter(g)
+        for later in ahead[g]:
+            relay(later)
         if g:
             finish(g - 1)
-        compute(g)
+        leave(g, hidden)
     finish(len(groups) - 1)
 
     for k in order:
@@ -189,11 +200,11 @@
     tok, width = tokens.shape
     hidden = gate_weight.shape[2]
     slots, cols = n * per, width // 2
-    groups = groups_of(n)
+    groups, ahead, sending = groups_of(n)
     any_spec, vmem_spec = pl.BlockSpec(memory_space=pl.ANY), pl.BlockSpec(memory_space=pltpu.VMEM)
     dma = pltpu.SemaphoreType.DMA
     returned, combine = pl.pallas_call(
-        functools.partial(kernel, n, per, groups),
+        functools.partial(kernel, n, per, groups, ahead, sending),
         out_shape=(
             pltpu.VMEM((slots, cols), BF16), pltpu.VMEM((tok, slots), BF16),
         ),

time: 32.2 us -> 32 us (level)
  the two profiles are of different devices: /device:TPU:0 before, /device:TPU:10 now
where the time goes in v4:
time: 32 us; the launch traced here: 31.8 us
  Pallas kernels  30.7 us (96%)
  matrix products  1.1 us (3%)
    pallas_call x1, Pallas kernels, per_device(): pl.pallas_call(functools.partial(kernel, n, per, groups, ahead, sending),...  30.7 us
    dot_general x1, matrix products, per_device(): return jnp.dot(combine, returned, preferred_element_type=F32).astype(BF16)  1.1 us

profile of v4, /device:TPU:10, one launch (start us, length us, event | category | flops | bytes accessed | tf_op | source)
XLA Modules:
  0.0 31.8 jit_solution(13611367092823358459)
XLA Ops:
  0.0 30.7 %shard_map.64 = (bf16[256,1024]{1,0:T(8,128)(2,1)S(1)}, bf16[256,256]{1,0:T(8,128)(2,1)S(1)}) custom-call(bf16[256,2048]{1,0:T(8,128)(2,1)} %tokens_hbm.1, s32[8,32]{1,0:T(8,128)} %picks_hbm.1, bf16[8,32]{1,0:T(8,128)(2,1)} %route_hbm.1, bf16[1,2048,512]{2,1,0:T(8,128)(2,1)} %gate_hbm.1, bf16[1,2048,512]{2,1,0:T(8,128)(2,1)} %up_hbm.1, ...), custom_call_target="tpu_custom_call" | custom-call | tf_op jit(solution)/shard_map/pallas_call | solution.py:206
  30.7 1.1 %convolution_convert_fusion = bf16[256,1024]{1,0:T(8,128)(2,1)} fusion(bf16[256,256]{1,0:T(8,128)(2,1)S(1)} %get-tuple-element.7, bf16[256,1024]{1,0:T(8,128)(2,1)S(1)} %get-tuple-element.8), kind=kOutput, calls=%fused_computation | convolution fusion | flops 134479872 | bytes 1179648 | tf_op jit(solution)/shard_map/dot_general | solution.py:235
